TPU v7x, 32 devices: a whole 2x2x4 slice. The times are simulated.
32 devices in a mesh: fs: 4 (over y, x), tp: 8 (over z, core).
Axes of the slice: x: 2, y: 2, z: 4, core: 2. Of those that a mesh axis runs over, the one named last changes fastest.
Arguments:
- tokens: bfloat16 [2048, 2048], P('fs', 'tp'), may hold values from -6 to 6
- norm_gain: float32 [2048], P('fs'), may hold values from 0.1 to 1.9
- gate_train: float32 [2048, 8192], P('fs', 'tp'), may hold values from -0.125 to 0.125
- up_train: float32 [2048, 8192], P('fs', 'tp'), may hold values from -0.125 to 0.125
- down_train: float32 [8192, 2048], P('fs', 'tp'), may hold values from -0.0625 to 0.0625
Outputs:
- gate_serve: bfloat16 [2048, 8192], P(None, 'tp')
- up_serve: bfloat16 [2048, 8192], P(None, 'tp')
- down_serve: bfloat16 [8192, 2048], P('tp')
- layer_out: bfloat16 [2048, 2048], P(('fs', 'tp'))
All inputs are finite; a program needn't handle non-finite values.
Results may differ from a plain program's by a relative error of at most 0.024.
Values may be sent and summed in bfloat16 or wider, within the bound.
A program may use at most 64 MiB of HBM per device.

v0:
```python
import jax
import jax.numpy as jnp
from jax import lax
from jax.sharding import PartitionSpec as P

D = 2048
epsilon = 1e-06


def body(tokens, norm_gain, gate_train, up_train, down_train):
    gate_local = (norm_gain[:, None] * gate_train).astype(jnp.bfloat16)
    up_local = (norm_gain[:, None] * up_train).astype(jnp.bfloat16)
    down_local = down_train.astype(jnp.bfloat16)
    features = lax.all_gather(tokens, "tp", axis=1, tiled=True)
    wide = features.astype(jnp.float32)
    squares = jnp.sum(wide * wide, axis=1)
    gate_whole, up_whole = (
        lax.all_gather(gate_local, "fs", axis=0, tiled=True),
        lax.all_gather(up_local, "fs", axis=0, tiled=True),
    )
    gate_sum = jnp.dot(features, gate_whole, preferred_element_type=jnp.float32)
    up_sum = jnp.dot(features, up_whole, preferred_element_type=jnp.float32)
    down_rows = lax.all_gather(down_local, "fs", axis=0, tiled=True)
    down_whole = lax.all_to_all(down_rows, "tp", split_axis=0, concat_axis=1, tiled=True)
    scale = lax.rsqrt(squares / D + epsilon)[:, None]
    hidden = (jax.nn.silu(gate_sum * scale) * (up_sum * scale)).astype(jnp.bfloat16)
    mixed = lax.psum_scatter(
        jnp.dot(hidden, down_whole, preferred_element_type=jnp.float32).astype(jnp.bfloat16),
        "tp",
        scatter_dimension=0,
        tiled=True,
    )
    return (gate_whole, up_whole, down_whole, mixed)


def solution(mesh):
    return jax.shard_map(
        body,
        mesh=mesh,
        in_specs=(P("fs", "tp"), P("fs"), P("fs", "tp"), P("fs", "tp"), P("fs", "tp")),
        out_specs=(P(None, "tp"), P(None, "tp"), P("tp", None), P(("fs", "tp"), None)),
        check_vma=False,
    )
```

profile of v0, /device:TPU:0, one launch (start us, length us, event | category | flops | bytes accessed | tf_op | source)
XLA Modules:
  0.0 293.7 jit_solution(2137613969868247611)
XLA Ops:
  7.2 0.0 copy-start.2
  7.2 0.0 copy-start.3
  7.2 0.0 all-gather.9.cloned.1.call-start
  7.2 2.8 convert_element_type.20
  10.0 0.0 all-gather.9.cloned.1.call-update
  10.1 0.0 all-gather.11.cloned.1.call-start
  10.1 0.7 all-gather.11.cloned.1.call-update
  10.8 0.0 all-gather.5.cloned.1.call-start
  10.9 0.0 copy-done.2
  10.9 0.0 copy-done.3
  10.9 3.2 %multiply_convert_fusion = (bf16[512,1024]{1,0:T(8,128)(2,1)}, bf16[512,1024]{1,0:T(8,128)(2,1)}) fusion(f32[512,1024]{1,0:T(8,128)S(1)} %copy-done.2, f32[512]{0:T(512)S(1)} %copy-done.3, f32[512,1024]{1,0:T(8,128)} %param.7), kind=kLoop, calls=%fused_computation.9 | loop fusion | flops 2097152 | bytes 6293504 | tf_op jit(solution)/shard_map/convert_element_type | solution.py:12
  14.1 0.0 all-gather.5.cloned.1.call-update
  14.1 51.6 %all-gather.9.cloned.1.call-done = bf16[8192,256]{1,0:T(8,128)(2,1)} async-done(((bf16[2048,256]{1,0:T(8,128)(2,1)}), bf16[8192,256]{1,0:T(8,128)(2,1)}) %all-gather.9.cloned.1.call-update) | async-done | bytes 4194320 | tf_op jit(solution)/shard_map/all_gather | solution.py:23
  65.7 4.6 %all-to-all-start = ((bf16[8,1024,256]{2,1,0:T(8,128)(2,1)}), bf16[8,1024,256]{2,1,0:T(8,128)(2,1)}, u32[]{:S(2)}, u32[]{:S(2)}) async-start(bf16[8,1024,256]{2,1,0:T(8,128)(2,1)} %bitcast.32), calls=%async_computation | async-start | bytes 8388608 | tf_op jit(solution)/shard_map/all_to_all | solution.py:24
  70.3 0.0 all-gather.7.cloned.1.call-start
  70.4 0.5 all-gather.7.cloned.1.call-update
  70.9 0.0 reduce-scatter.2.cloned.1.call-start
  71.0 50.9 %all-gather.11.cloned.1.call-done = bf16[512,2048]{1,0:T(8,128)(2,1)} async-done(((bf16[512,256]{1,0:T(8,128)(2,1)}), bf16[512,2048]{1,0:T(8,128)(2,1)}) %all-gather.11.cloned.1.call-update) | async-done | bytes 2097168 | tf_op jit(solution)/shard_map/all_gather | solution.py:14
  121.8 0.0 copy-start.1
  121.8 2.2 multiply_reduce_fusion
  124.1 54.8 %all-gather.5.cloned.1.call-done = bf16[2048,1024]{1,0:T(8,128)(2,1)} async-done(((bf16[512,1024]{1,0:T(8,128)(2,1)}), bf16[2048,1024]{1,0:T(8,128)(2,1)}) %all-gather.5.cloned.1.call-update) | async-done | bytes 4194320 | tf_op jit(solution)/shard_map/all_gather | solution.py:18
  178.9 0.0 copy-done.1
  178.9 5.9 %fusion.5 = f32[1024,512]{1,0:T(8,128)} fusion(bf16[2048,1024]{1,0:T(8,128)(2,1)} %all-gather.5.cloned.1.call-done, bf16[512,2048]{1,0:T(8,128)(2,1)S(1)} %copy-done.1), kind=kOutput, calls=%fused_computation.13 | convolution fusion | flops 2147483648 | bytes 8388608 | tf_op jit(solution)/shard_map/dot_general | solution.py:21
  184.8 0.0 all-to-all-done
  184.8 6.5 %copy.10 = bf16[8,1024,256]{1,2,0:T(8,128)(2,1)} copy(bf16[8,1024,256]{2,1,0:T(8,128)(2,1)} %all-to-all-done) | data formatting | bytes 8388608 | tf_op jit(solution)/shard_map/all_to_all | solution.py:24
  191.2 42.5 %all-gather.7.cloned.1.call-done = bf16[2048,1024]{1,0:T(8,128)(2,1)} async-done(((bf16[512,1024]{1,0:T(8,128)(2,1)}), bf16[2048,1024]{1,0:T(8,128)(2,1)}) %all-gather.7.cloned.1.call-update) | async-done | bytes 4194320 | tf_op jit(solution)/shard_map/all_gather | solution.py:19
  233.7 10.3 %convolution_convert_fusion = bf16[512,2048]{1,0:T(8,128)(2,1)} fusion(bf16[1024,2048]{0,1:T(8,128)(2,1)} %bitcast.30, f32[1024,512]{1,0:T(8,128)} %fusion.5, bf16[2048,1024]{1,0:T(8,128)(2,1)} %all-gather.7.cloned.1.call-done, bf16[512,2048]{1,0:T(8,128)(2,1)S(1)} %copy-done.1, f32[512]{0:T(512)S(1)} %add_rsqrt_fusion), kind=kOutput, calls=%fused_computation.1 | convolution fusion | flops 4300210176 | bytes 14682112 | tf_op jit(solution)/shard_map/dot_general | solution.py:28
  244.0 0.0 reduce-scatter.2.cloned.1.call-update
  244.0 6.4 %copy.11 = bf16[1024,2048]{1,0:T(8,128)(2,1)} copy(bf16[1024,2048]{0,1:T(8,128)(2,1)} %bitcast.31) | data formatting | bytes 8388608
  250.5 29.8 %reduce-scatter.2.cloned.1.call-done = bf16[64,2048]{1,0:T(8,128)(2,1)} async-done(((bf16[512,2048]{1,0:T(8,128)(2,1)}), bf16[64,2048]{1,0:T(8,128)(2,1)}) %reduce-scatter.2.cloned.1.call-update) | async-done | bytes 262160 | tf_op jit(solution)/shard_map/reduce_scatter | solution.py:27
  280.3 0.0 copy-start
  280.3 4.8 %copy.14 = bf16[2048,1024]{1,0:T(8,128)(2,1)} copy(bf16[2048,1024]{1,0:T(8,128)(2,1)} %all-gather.5.cloned.1.call-done) | data formatting | bytes 8388608
  285.1 0.0 copy-done
  285.1 2.0 copy.15
  (1 shorter events, 0.0 us)
Async XLA Ops:
  7.2 3.7 %copy-start.2 = (f32[512,1024]{1,0:T(8,128)S(1)}, f32[512,1024]{1,0:T(8,128)}, u32[]{:S(2)}) copy-start(f32[512,1024]{1,0:T(8,128)} %param.8) | copy-start | bytes 6291460
  7.2 3.7 %copy-start.3 = (f32[512]{0:T(512)S(1)}, f32[512]{0:T(512)}, u32[]{:S(2)}) copy-start(f32[512]{0:T(512)} %param.6) | copy-start | bytes 6148
  7.2 58.6 %all-gather.9.cloned.1.call-start = ((), (), s32[]{:S(2)}) async-start(), calls=%async_computation.4 | async-start | bytes 5242880 | tf_op jit(solution)/shard_map/all_gather | solution.py:23
  10.1 111.8 %all-gather.11.cloned.1.call-start = ((), (), s32[]{:S(2)}) async-start(), calls=%async_computation.5 | async-start | bytes 2359296 | tf_op jit(solution)/shard_map/all_gather | solution.py:14
  10.8 168.1 %all-gather.5.cloned.1.call-start = ((), (), s32[]{:S(2)}) async-start(), calls=%async_computation.2 | async-start | bytes 5242880 | tf_op jit(solution)/shard_map/all_gather | solution.py:18
  65.7 119.0 %all-to-all-start = ((bf16[8,1024,256]{2,1,0:T(8,128)(2,1)}), bf16[8,1024,256]{2,1,0:T(8,128)(2,1)}, u32[]{:S(2)}, u32[]{:S(2)}) async-start(bf16[8,1024,256]{2,1,0:T(8,128)(2,1)} %bitcast.32), calls=%async_computation | async-start | bytes 8388608 | tf_op jit(solution)/shard_map/all_to_all | solution.py:24
  70.3 163.4 %all-gather.7.cloned.1.call-start = ((), (), s32[]{:S(2)}) async-start(), calls=%async_computation.3 | async-start | bytes 5242880 | tf_op jit(solution)/shard_map/all_gather | solution.py:19
  70.9 209.4 %reduce-scatter.2.cloned.1.call-start = ((), (), s32[]{:S(2)}) async-start(), calls=%async_computation.6 | async-start | bytes 2359296 | tf_op jit(solution)/shard_map/reduce_scatter | solution.py:27
  121.8 57.0 %copy-start.1 = (bf16[512,2048]{1,0:T(8,128)(2,1)S(1)}, bf16[512,2048]{1,0:T(8,128)(2,1)}, u32[]{:S(2)}) copy-start(bf16[512,2048]{1,0:T(8,128)(2,1)} %all-gather.11.cloned.1.call-done) | copy-start | bytes 6291460
  280.3 4.8 %copy-start = (bf16[2048,1024]{1,0:T(8,128)(2,1)S(1)}, bf16[2048,1024]{1,0:T(8,128)(2,1)}, u32[]{:S(2)}) copy-start(bf16[2048,1024]{1,0:T(8,128)(2,1)} %all-gather.7.cloned.1.call-done) | copy-start | bytes 12582916
Sparse Core Ops, SparseCore 0:
  10.4 55.2 all-gather.8
  67.3 54.4 all-gather.10
  124.3 54.5 all-gather.4
  181.1 52.5 all-gather.6
  244.2 36.0 reduce-scatter.1
where the time goes:
time: 294 us
  waiting for transfers between devices  231 us (79%)
  local copies, waits for them, and re-layouts  19.8 us (7%)
  matrix products  16.2 us (6%)
  between operations  13.8 us (5%)
  other arithmetic  8.23 us (3%)
  starting transfers between devices  4.8 us (2%)
    all_gather x1, waiting for transfers between devices, body(): lax.all_gather(gate_local, 'fs', axis=0, tiled=True)  54.8 us
    all_gather x1, waiting for transfers between devices, body(): down_rows = lax.all_gather(down_local, 'fs', axis=0, tiled=True)  51.6 us
    all_gather x1, waiting for transfers between devices, body(): features = lax.all_gather(tokens, 'tp', axis=1, tiled=True)  50.9 us
    all_gather x1, waiting for transfers between devices, body(): lax.all_gather(up_local, 'fs', axis=0, tiled=True)  42.5 us
    reduce_scatter x1, waiting for transfers between devices, body(): lax.psum_scatter(jnp.dot(hidden, down_whole, preferred_element_type=jnp.f...  29.8 us
    unnamed x11, local copies, waits for them, and re-layouts  13.3 us
    dot_general x1, matrix products, body(): jnp.dot(hidden, down_whole, preferred_element_type=jnp.float32)  10.3 us
    all_to_all x1, local copies, waits for them, and re-layouts, body(): lax.all_to_all(down_rows, 'tp', split_axis=0, concat_axis=1, tiled=True)  6.48 us
  transfers between devices with their start and end apart: 6, of which 5 were waited for; matrix products, arithmetic and copies ran while one was open for 8% of the time, Pallas kernels for 0%

commit v1 on v0

--- a/solution.py
+++ b/solution.py
@@ -11,7 +11,15 @@
     gate_local = (norm_gain[:, None] * gate_train).astype(jnp.bfloat16)
     up_local = (norm_gain[:, None] * up_train).astype(jnp.bfloat16)
     down_local = down_train.astype(jnp.bfloat16)
-    features = lax.all_gather(tokens, "tp", axis=1, tiled=True)
+    devices, here, span = (lax.axis_size("tp"), lax.axis_index("tp"), tokens.shape[1])
+    forward = [(i, (i + 1) % devices) for i in range(devices)]
+    features = jnp.zeros((*tokens.shape[:1], devices * span, *tokens.shape[1 + 1 :]), tokens.dtype)
+    carried = tokens
+    for step in range(devices):
+        owner = (here - step) % devices
+        features = lax.dynamic_update_slice_in_dim(features, carried, owner * span, axis=1)
+        if step < devices - 1:
+            carried = lax.ppermute(carried, "tp", forward)
     wide = features.astype(jnp.float32)
     squares = jnp.sum(wide * wide, axis=1)
     gate_whole, up_whole = (

time: 294 us -> 272 us (0.925)
  waiting for transfers between devices: 231 us -> 193 us
  starting transfers between devices: 4.8 us -> 22.6 us
    ppermute x0 -> x7, waiting for transfers between devices: none -> 105 us  [body(): carried = lax.ppermute(carried, 'tp', forward)]
    all_gather x1, waiting for transfers between devices: 54.8 us -> 0.02 us  [body(): lax.all_gather(gate_local, 'fs', axis=0, tiled=True)]
    all_gather x1 -> x0, waiting for transfers between devices: 50.9 us -> none  [body(): features = lax.all_gather(tokens, 'tp', axis=1, tiled=True)]
    all_gather x1, waiting for transfers between devices: 42.5 us -> 0.01 us  [body(): lax.all_gather(up_local, 'fs', axis=0, tiled=True)]
    ppermute x0 -> x7, starting transfers between devices: none -> 17.7 us  [body(): carried = lax.ppermute(carried, 'tp', forward)]
    reduce_scatter x1, waiting for transfers between devices: 29.8 us -> 34.2 us  [body(): lax.psum_scatter(jnp.dot(hidden, down_whole, preferred_element_type=jnp.f...]
    unnamed x11 -> x15, local copies, waits for them, and re-layouts: 13.3 us -> 13.3 us
  transfers between devices with their start and end apart: 6 -> 12, of which waited for: 5 -> 9; matrix products, arithmetic and copies ran while one was open for 8% -> 8% of each run, Pallas kernels for 0% -> 0%
where the time goes in v1:
time: 272 us
  waiting for transfers between devices  193 us (71%)
  starting transfers between devices  22.6 us (8%)
  local copies, waits for them, and re-layouts  20.2 us (7%)
  matrix products  15.9 us (6%)
  between operations  13.9 us (5%)
  other arithmetic  6.5 us (2%)
    ppermute x7, waiting for transfers between devices, body(): carried = lax.ppermute(carried, 'tp', forward)  105 us
    all_gather x1, waiting for transfers between devices, body(): down_rows = lax.all_gather(down_local, 'fs', axis=0, tiled=True)  52.4 us
    reduce_scatter x1, waiting for transfers between devices, body(): lax.psum_scatter(jnp.dot(hidden, down_whole, preferred_element_type=jnp.f...  34.2 us
    ppermute x7, starting transfers between devices, body(): carried = lax.ppermute(carried, 'tp', forward)  17.7 us
    unnamed x15, local copies, waits for them, and re-layouts  13.3 us
    dot_general x1, matrix products, body(): jnp.dot(hidden, down_whole, preferred_element_type=jnp.float32)  10.1 us
    all_to_all x1, local copies, waits for them, and re-layouts, body(): lax.all_to_all(down_rows, 'tp', split_axis=0, concat_axis=1, tiled=True)  6.43 us
    dot_general x1, matrix products, body(): gate_sum = jnp.dot(features, gate_whole, preferred_element_type=jnp.float32)  5.84 us
  transfers between devices with their start and end apart: 12, of which 9 were waited for; matrix products, arithmetic and copies ran while one was open for 8% of the time, Pallas kernels for 0%

profile of v1, /device:TPU:0, one launch (start us, length us, event | category | flops | bytes accessed | tf_op | source)
XLA Modules:
  0.0 271.6 jit_solution(8709022535425657729)
XLA Ops:
  7.2 0.0 copy-start.1
  7.2 0.0 copy-start.5
  7.2 0.0 all-gather.8.cloned.1.call-start
  7.2 2.8 %convert_element_type.20 = bf16[2048,256]{1,0:T(8,128)(2,1)} convert(f32[2048,256]{1,0:T(8,128)} %param.9) | non-fusion elementwise | flops 524288 | bytes 3145728 | tf_op jit(solution)/shard_map/convert_element_type | solution.py:13
  10.0 0.0 all-gather.8.cloned.1.call-update
  10.1 0.0 all-gather.4.cloned.1.call-start
  10.1 0.0 copy-done.1
  10.1 0.0 copy-done.5
  10.1 3.2 %multiply_convert_fusion.1 = (bf16[512,1024]{1,0:T(8,128)(2,1)}, bf16[512,1024]{1,0:T(8,128)(2,1)}) fusion(f32[512,1024]{1,0:T(8,128)S(1)} %copy-done.1, f32[512]{0:T(512)S(1)} %copy-done.5, f32[512,1024]{1,0:T(8,128)} %param.7), kind=kLoop, calls=%fused_computation.3 | loop fusion | flops 2097152 | bytes 6293504 | tf_op jit(solution)/shard_map/convert_element_type | solution.py:12
  13.3 0.0 all-gather.4.cloned.1.call-update
  13.4 52.4 %all-gather.8.cloned.1.call-done = bf16[8192,256]{1,0:T(8,128)(2,1)} async-done(((bf16[2048,256]{1,0:T(8,128)(2,1)}), bf16[8192,256]{1,0:T(8,128)(2,1)}) %all-gather.8.cloned.1.call-update) | async-done | bytes 4194320 | tf_op jit(solution)/shard_map/all_gather | solution.py:31
  65.7 0.0 copy-start.2
  65.7 4.7 %all-to-all-start = ((bf16[8,1024,256]{2,1,0:T(8,128)(2,1)}), bf16[8,1024,256]{2,1,0:T(8,128)(2,1)}, u32[]{:S(2)}, u32[]{:S(2)}) async-start(bf16[8,1024,256]{2,1,0:T(8,128)(2,1)} %bitcast.11), calls=%async_computation | async-start | bytes 8388608 | tf_op jit(solution)/shard_map/all_to_all | solution.py:32
  70.5 0.0 all-gather.6.cloned.1.call-start
  70.5 0.7 all-gather.6.cloned.1.call-update
  71.2 0.0 reduce-scatter.2.cloned.1.call-start
  71.3 0.0 copy-done.2
  71.3 0.5 collective-permute-start
  71.8 74.0 %collective-permute-done = bf16[512,256]{1,0:T(8,128)(2,1)S(1)} collective-permute-done((bf16[512,256]{1,0:T(8,128)(2,1)S(1)}, bf16[512,256]{1,0:T(8,128)(2,1)S(1)}, u32[]{:S(2)}, u32[]{:S(2)}) %collective-permute-start) | collective-permute-done | bytes 262176 | tf_op jit(solution)/shard_map/ppermute | solution.py:22
  145.8 0.0 collective-permute-start.1
  145.8 7.7 %collective-permute-done.1 = bf16[512,256]{1,0:T(8,128)(2,1)S(1)} collective-permute-done((bf16[512,256]{1,0:T(8,128)(2,1)S(1)}, bf16[512,256]{1,0:T(8,128)(2,1)S(1)}, u32[]{:S(2)}, u32[]{:S(2)}) %collective-permute-start.1) | collective-permute-done | bytes 262176 | tf_op jit(solution)/shard_map/ppermute | solution.py:22
  153.5 0.0 collective-permute-start.2
  153.5 7.7 %collective-permute-done.2 = bf16[512,256]{1,0:T(8,128)(2,1)S(1)} collective-permute-done((bf16[512,256]{1,0:T(8,128)(2,1)S(1)}, bf16[512,256]{1,0:T(8,128)(2,1)S(1)}, u32[]{:S(2)}, u32[]{:S(2)}) %collective-permute-start.2) | collective-permute-done | bytes 262176 | tf_op jit(solution)/shard_map/ppermute | solution.py:22
  161.2 0.0 copy-start.3
  161.2 9.2 %collective-permute-start.3 = (bf16[512,256]{1,0:T(8,128)(2,1)S(1)}, bf16[512,256]{1,0:T(8,128)(2,1)S(1)}, u32[]{:S(2)}, u32[]{:S(2)}) collective-permute-start(bf16[512,256]{1,0:T(8,128)(2,1)S(1)} %collective-permute-done.2), channel_id=1, source_target_pairs={{0,1},{1,2},{2,3},{3,4},{4,5},{5,6},{6,7},{7,0},{8,9},{9,10},{10,1... | collective-permute-start | bytes 786440 | tf_op jit(solution)/shard_map/ppermute | solution.py:22
  170.5 1.2 collective-permute-done.3
  171.6 0.0 copy-done.3
  171.6 4.6 %collective-permute-start.4 = (bf16[512,256]{1,0:T(8,128)(2,1)S(1)}, bf16[512,256]{1,0:T(8,128)(2,1)S(1)}, u32[]{:S(2)}, u32[]{:S(2)}) collective-permute-start(bf16[512,256]{1,0:T(8,128)(2,1)S(1)} %collective-permute-done.3), channel_id=1, source_target_pairs={{0,1},{1,2},{2,3},{3,4},{4,5},{5,6},{6,7},{7,0},{8,9},{9,10},{10,1... | collective-permute-start | bytes 786440 | tf_op jit(solution)/shard_map/ppermute | solution.py:22
  176.3 0.0 copy-start.4
  176.3 0.2 broadcast_in_dim.2
  176.5 3.0 %collective-permute-done.4 = bf16[512,256]{1,0:T(8,128)(2,1)S(1)} collective-permute-done((bf16[512,256]{1,0:T(8,128)(2,1)S(1)}, bf16[512,256]{1,0:T(8,128)(2,1)S(1)}, u32[]{:S(2)}, u32[]{:S(2)}) %collective-permute-start.4) | collective-permute-done | bytes 262176 | tf_op jit(solution)/shard_map/ppermute | solution.py:22
  179.5 2.5 collective-permute-start.5
  182.1 0.0 copy-done.4
  182.2 4.9 %collective-permute-done.5 = bf16[512,256]{1,0:T(8,128)(2,1)S(1)} collective-permute-done((bf16[512,256]{1,0:T(8,128)(2,1)S(1)}, bf16[512,256]{1,0:T(8,128)(2,1)S(1)}, u32[]{:S(2)}, u32[]{:S(2)}) %collective-permute-start.5) | collective-permute-done | bytes 262176 | tf_op jit(solution)/shard_map/ppermute | solution.py:22
  187.1 0.7 collective-permute-start.6
  188.0 6.8 %collective-permute-done.6 = bf16[512,256]{1,0:T(8,128)(2,1)S(1)} collective-permute-done((bf16[512,256]{1,0:T(8,128)(2,1)S(1)}, bf16[512,256]{1,0:T(8,128)(2,1)S(1)}, u32[]{:S(2)}, u32[]{:S(2)}) %collective-permute-start.6) | collective-permute-done | bytes 262176 | tf_op jit(solution)/shard_map/ppermute | solution.py:22
  194.7 0.5 multiply_reduce_fusion
  195.2 0.0 all-gather.4.cloned.1.call-done
  195.3 5.8 %fusion.1 = f32[512,1024]{1,0:T(8,128)} fusion(bf16[512,2048]{1,0:T(8,128)(2,1)S(1)} %constant_dynamic-update-slice_fusion, bf16[2048,1024]{1,0:T(8,128)(2,1)} %all-gather.4.cloned.1.call-done), kind=kOutput, calls=%fused_computation.15 | convolution fusion | flops 2147483648 | bytes 8388608 | tf_op jit(solution)/shard_map/dot_general | solution.py:29
  201.1 0.0 all-to-all-done
  201.1 6.4 %copy.10 = bf16[8,1024,256]{1,2,0:T(8,128)(2,1)} copy(bf16[8,1024,256]{2,1,0:T(8,128)(2,1)} %all-to-all-done) | data formatting | bytes 8388608 | tf_op jit(solution)/shard_map/all_to_all | solution.py:32
  207.5 10.1 %convolution_convert_fusion = bf16[512,2048]{1,0:T(8,128)(2,1)} fusion(bf16[1024,2048]{0,1:T(8,128)(2,1)} %bitcast.9, f32[512,1024]{1,0:T(8,128)} %fusion.1, bf16[512,2048]{1,0:T(8,128)(2,1)S(1)} %constant_dynamic-update-slice_fusion, bf16[2048,1024]{1,0:T(8,128)(2,1)} %all-gather.6.cloned.1.call-done, f32[512]{0:T(512)S(1)} %add_rsqrt_fusion), kind=kOutput, calls=%fused_computation.1 | convolution fusion | flops 4300210176 | bytes 14682112 | tf_op jit(solution)/shard_map/dot_general | solution.py:36
  217.6 0.0 reduce-scatter.2.cloned.1.call-update
  217.6 6.4 %copy.11 = bf16[1024,2048]{1,0:T(8,128)(2,1)} copy(bf16[1024,2048]{0,1:T(8,128)(2,1)} %bitcast.10) | data formatting | bytes 8388608
  224.1 34.2 %reduce-scatter.2.cloned.1.call-done = bf16[64,2048]{1,0:T(8,128)(2,1)} async-done(((bf16[512,2048]{1,0:T(8,128)(2,1)}), bf16[64,2048]{1,0:T(8,128)(2,1)}) %reduce-scatter.2.cloned.1.call-update) | async-done | bytes 262160 | tf_op jit(solution)/shard_map/reduce_scatter | solution.py:35
  258.3 4.8 %copy.22 = bf16[2048,1024]{1,0:T(8,128)(2,1)} copy(bf16[2048,1024]{1,0:T(8,128)(2,1)} %all-gather.4.cloned.1.call-done) | data formatting | bytes 8388608
  263.1 0.0 copy-done
  263.1 2.0 copy.23
  (11 shorter events, 0.2 us)
Async XLA Ops:
  7.2 2.9 %copy-start.1 = (f32[512,1024]{1,0:T(8,128)S(1)}, f32[512,1024]{1,0:T(8,128)}, u32[]{:S(2)}) copy-start(f32[512,1024]{1,0:T(8,128)} %param.8) | copy-start | bytes 6291460
  7.2 2.9 %copy-start.5 = (f32[512]{0:T(512)S(1)}, f32[512]{0:T(512)}, u32[]{:S(2)}) copy-start(f32[512]{0:T(512)} %param.6) | copy-start | bytes 6148
  7.2 58.6 %all-gather.8.cloned.1.call-start = ((), (), s32[]{:S(2)}) async-start(), calls=%async_computation.4 | async-start | bytes 5242880 | tf_op jit(solution)/shard_map/all_gather | solution.py:31
  10.1 185.2 %all-gather.4.cloned.1.call-start = ((), (), s32[]{:S(2)}) async-start(), calls=%async_computation.2 | async-start | bytes 5242880 | tf_op jit(solution)/shard_map/all_gather | solution.py:26
  65.7 5.5 %copy-start.2 = (bf16[512,256]{1,0:T(8,128)(2,1)S(1)}, bf16[512,256]{1,0:T(8,128)(2,1)}, u32[]{:S(2)}) copy-start(bf16[512,256]{1,0:T(8,128)(2,1)} %param.5) | copy-start | bytes 786436
  65.7 135.4 %all-to-all-start = ((bf16[8,1024,256]{2,1,0:T(8,128)(2,1)}), bf16[8,1024,256]{2,1,0:T(8,128)(2,1)}, u32[]{:S(2)}, u32[]{:S(2)}) async-start(bf16[8,1024,256]{2,1,0:T(8,128)(2,1)} %bitcast.11), calls=%async_computation | async-start | bytes 8388608 | tf_op jit(solution)/shard_map/all_to_all | solution.py:32
  70.5 137.1 %all-gather.6.cloned.1.call-start = ((), (), s32[]{:S(2)}) async-start(), calls=%async_computation.3 | async-start | bytes 5242880 | tf_op jit(solution)/shard_map/all_gather | solution.py:27
  71.2 187.1 %reduce-scatter.2.cloned.1.call-start = ((), (), s32[]{:S(2)}) async-start(), calls=%async_computation.5 | async-start | bytes 2359296 | tf_op jit(solution)/shard_map/reduce_scatter | solution.py:35
  71.3 74.6 %collective-permute-start = (bf16[512,256]{1,0:T(8,128)(2,1)S(1)}, bf16[512,256]{1,0:T(8,128)(2,1)S(1)}, u32[]{:S(2)}, u32[]{:S(2)}) collective-permute-start(bf16[512,256]{1,0:T(8,128)(2,1)S(1)} %copy-done.2), channel_id=1, source_target_pairs={{0,1},{1,2},{2,3},{3,4},{4,5},{5,6},{6,7},{7,0},{8,9},{9,10},{10,1... | collective-permute-start | bytes 786440 | tf_op jit(solution)/shard_map/ppermute | solution.py:22
  145.8 7.7 %collective-permute-start.1 = (bf16[512,256]{1,0:T(8,128)(2,1)S(1)}, bf16[512,256]{1,0:T(8,128)(2,1)S(1)}, u32[]{:S(2)}, u32[]{:S(2)}) collective-permute-start(bf16[512,256]{1,0:T(8,128)(2,1)S(1)} %collective-permute-done), channel_id=1, source_target_pairs={{0,1},{1,2},{2,3},{3,4},{4,5},{5,6},{6,7},{7,0},{8,9},{9,10},{10,1... | collective-permute-start | bytes 786440 | tf_op jit(solution)/shard_map/ppermute | solution.py:22
  153.5 7.7 %collective-permute-start.2 = (bf16[512,256]{1,0:T(8,128)(2,1)S(1)}, bf16[512,256]{1,0:T(8,128)(2,1)S(1)}, u32[]{:S(2)}, u32[]{:S(2)}) collective-permute-start(bf16[512,256]{1,0:T(8,128)(2,1)S(1)} %collective-permute-done.1), channel_id=1, source_target_pairs={{0,1},{1,2},{2,3},{3,4},{4,5},{5,6},{6,7},{7,0},{8,9},{9,10},{10,1... | collective-permute-start | bytes 786440 | tf_op jit(solution)/shard_map/ppermute | solution.py:22
  161.2 10.4 %copy-start.3 = (bf16[512,256]{1,0:T(8,128)(2,1)}, bf16[512,256]{1,0:T(8,128)(2,1)S(1)}, u32[]{:S(2)}) copy-start(bf16[512,256]{1,0:T(8,128)(2,1)S(1)} %collective-permute-done.2) | copy-start | bytes 786436
  161.2 10.4 %collective-permute-start.3 = (bf16[512,256]{1,0:T(8,128)(2,1)S(1)}, bf16[512,256]{1,0:T(8,128)(2,1)S(1)}, u32[]{:S(2)}, u32[]{:S(2)}) collective-permute-start(bf16[512,256]{1,0:T(8,128)(2,1)S(1)} %collective-permute-done.2), channel_id=1, source_target_pairs={{0,1},{1,2},{2,3},{3,4},{4,5},{5,6},{6,7},{7,0},{8,9},{9,10},{10,1... | collective-permute-start | bytes 786440 | tf_op jit(solution)/shard_map/ppermute | solution.py:22
  171.6 7.9 %collective-permute-start.4 = (bf16[512,256]{1,0:T(8,128)(2,1)S(1)}, bf16[512,256]{1,0:T(8,128)(2,1)S(1)}, u32[]{:S(2)}, u32[]{:S(2)}) collective-permute-start(bf16[512,256]{1,0:T(8,128)(2,1)S(1)} %collective-permute-done.3), channel_id=1, source_target_pairs={{0,1},{1,2},{2,3},{3,4},{4,5},{5,6},{6,7},{7,0},{8,9},{9,10},{10,1... | collective-permute-start | bytes 786440 | tf_op jit(solution)/shard_map/ppermute | solution.py:22
  176.3 5.9 %copy-start.4 = (bf16[512,256]{1,0:T(8,128)(2,1)S(1)}, bf16[512,256]{1,0:T(8,128)(2,1)}, u32[]{:S(2)}) copy-start(bf16[512,256]{1,0:T(8,128)(2,1)} %copy-done.3) | copy-start | bytes 786436
  179.5 7.6 %collective-permute-start.5 = (bf16[512,256]{1,0:T(8,128)(2,1)S(1)}, bf16[512,256]{1,0:T(8,128)(2,1)S(1)}, u32[]{:S(2)}, u32[]{:S(2)}) collective-permute-start(bf16[512,256]{1,0:T(8,128)(2,1)S(1)} %collective-permute-done.4), channel_id=1, source_target_pairs={{0,1},{1,2},{2,3},{3,4},{4,5},{5,6},{6,7},{7,0},{8,9},{9,10},{10,1... | collective-permute-start | bytes 786440 | tf_op jit(solution)/shard_map/ppermute | solution.py:22
  187.1 7.6 %collective-permute-start.6 = (bf16[512,256]{1,0:T(8,128)(2,1)S(1)}, bf16[512,256]{1,0:T(8,128)(2,1)S(1)}, u32[]{:S(2)}, u32[]{:S(2)}) collective-permute-start(bf16[512,256]{1,0:T(8,128)(2,1)S(1)} %collective-permute-done.5), channel_id=1, source_target_pairs={{0,1},{1,2},{2,3},{3,4},{4,5},{5,6},{6,7},{7,0},{8,9},{9,10},{10,1... | collective-permute-start | bytes 786440 | tf_op jit(solution)/shard_map/ppermute | solution.py:22
  258.3 4.8 %copy-start = (bf16[2048,1024]{1,0:T(8,128)(2,1)S(1)}, bf16[2048,1024]{1,0:T(8,128)(2,1)}, u32[]{:S(2)}) copy-start(bf16[2048,1024]{1,0:T(8,128)(2,1)} %all-gather.6.cloned.1.call-done) | copy-start | bytes 12582916
Sparse Core Ops, SparseCore 0:
  10.4 55.2 all-gather.7
  68.2 52.5 all-gather.3
  123.2 52.5 all-gather.5
  217.8 40.4 reduce-scatter.1
